TPU v7x, 32 devices: a whole 2x2x4 slice. The times are simulated.
32 devices in a mesh: kv: 16 (over z, y, core), tp: 2 (over x).
Axes of the slice: x: 2, y: 2, z: 4, core: 2. Of those that a mesh axis runs over, the one named last changes fastest.
Arguments:
- hidden_rows: bfloat16 [6144, 2048], P('kv'), may hold values from -6 to 6
- proj_query: bfloat16 [2048, 2048], P(None, 'tp'), may hold values from -0.125 to 0.125
- proj_key: bfloat16 [2048, 256], P(None, 'tp'), may hold values from -0.125 to 0.125
- proj_value: bfloat16 [2048, 256], P(None, 'tp'), may hold values from -0.125 to 0.125
- proj_output: bfloat16 [2048, 2048], P('tp'), may hold values from -0.125 to 0.125
- head_scale: float32 [32], P('tp'), may hold values from 0.25 to 96
- hot_blocks: int32 [16], replicated, may hold values from 0 to 191, as said below
- chosen_blocks: int32 [96, 16], P('kv'), may hold values from 0 to 27, as said below
Outputs:
- layer_out: bfloat16 [6144, 2048], P('kv', 'tp')
Inputs may be any that keep to these rules, and one draw needn't show every extreme that they name: `hot_blocks`: 16 different key-block numbers; no device's 12 key blocks hold more than 2 of them, and in every draw some device holds exactly 2. `chosen_blocks`: each row's 16 codes name different key blocks; among them are the key blocks that cover the positions of query block b; no code of 12 or more names a block on the query block's own device.
All inputs are finite; a program needn't handle non-finite values.
Results may differ from a plain program's by a relative error of at most 0.01.
The roundings to bfloat16 on the way count: a program that leaves them out, or rounds other values in their place, can miss the bound.
Values may be sent and summed in bfloat16 or wider, within the bound.
A program may use at most 64 MiB of HBM per device.

v0:
```python
import functools

import jax
import jax.numpy as jnp
from jax import lax
from jax.experimental import pallas as pl
from jax.experimental.pallas import tpu as pltpu
from jax.sharding import PartitionSpec as P

HD = 64
KB = 32
QB = 64
HOT_MOST = 2
LANES = 128
PIECES = 4
LOG2E = 1.4426950408889634
MESH = pl.DeviceIdType.MESH


def dot(a, b):
    return jnp.dot(a, b, preferred_element_type=jnp.float32)


def kernel(
    n,
    n_tp,
    x_hbm,
    wq_hbm,
    wk_hbm,
    wv_hbm,
    wo_hbm,
    scale_ref,
    hot_ref,
    chosen_ref,
    mine_hbm,
    got_hbm,
    x,
    wq,
    wk,
    wv,
    wo,
    q,
    local,
    pool,
    kvg,
    heads,
    sent,
    mine_part,
    slot_ref,
    load_sem,
    wq_sem,
    wo_sem,
    hot_send,
    pass_send,
    hot_recv,
    part_send,
    part_recv,
):
    me = lax.axis_index("kv")
    t = lax.axis_index("tp")
    own = local.shape[0]
    width = local.shape[2]
    nsel = chosen_ref.shape[1]
    nhot = hot_ref.shape[0]
    blocks = chosen_ref.shape[0]
    head_count = scale_ref.shape[0]
    kv_heads = wk.shape[1] // HD
    pairs = head_count // kv_heads // 2
    keys = nsel * KB
    part_cols = wo.shape[2]
    partner = me + 1 - 2 * lax.rem(me, 2)
    half = n // 2

    depth = x.shape[1] // PIECES
    cuts = [slice(i * depth, (i + 1) * depth) for i in range(PIECES)]
    loads = [
        [
            pltpu.make_async_copy(x_hbm.at[:, cut], x.at[:, cut], load_sem.at[3 * i]),
            pltpu.make_async_copy(wk_hbm.at[cut], wk.at[cut], load_sem.at[3 * i + 1]),
            pltpu.make_async_copy(wv_hbm.at[cut], wv.at[cut], load_sem.at[3 * i + 2]),
        ]
        for i, cut in enumerate(cuts)
    ]
    for piece in loads:
        for load in piece:
            load.start()
    q_chunk = wq.shape[2]
    wq_loads = [
        pltpu.make_async_copy(wq_hbm.at[:, pl.ds(i * q_chunk, q_chunk)], wq.at[i], wq_sem.at[i])
        for i in range(wq.shape[0])
    ]
    targets = [lax.rem(t + k, n_tp) for k in range(n_tp)]
    order = list(range(1, n_tp)) + [0]
    wo_loads = [
        pltpu.make_async_copy(
            wo_hbm.at[:, pl.ds(pl.multiple_of(targets[k] * part_cols, LANES), part_cols)],
            wo.at[k],
            wo_sem.at[k],
        )
        for k in range(n_tp)
    ]

    barrier = pltpu.get_barrier_semaphore()

    def greet(j, carry):
        pl.semaphore_signal(
            barrier, inc=1, device_id=(lax.rem(me + 2 * j, n), t), device_id_type=MESH
        )
        return carry

    lax.fori_loop(1, half, greet, 0)
    pl.semaphore_signal(barrier, inc=1, device_id=(partner, t), device_id_type=MESH)
    for k in range(1, n_tp):
        pl.semaphore_signal(barrier, inc=1, device_id=(me, targets[k]), device_id_type=MESH)

    hots = [hot_ref[h] for h in range(nhot)]
    owners = [lax.div(hot, own) for hot in hots]
    mine = [jnp.int32(0), jnp.int32(0)]
    for h in range(nhot):
        rank = jnp.int32(0)
        for g in range(h):
            rank = rank + (owners[g] == owners[h]).astype(jnp.int32)
        slot_ref[h] = own + owners[h] * HOT_MOST + rank
        offset = hots[h] - owners[h] * own
        for r in range(HOT_MOST):
            mine[r] = jnp.where((owners[h] == me) & (rank == r), offset, mine[r])

    total = None
    for piece, cut in zip(loads, cuts):
        for load in piece:
            load.wait()
        term = dot(x[:, cut], jnp.concatenate([wk[cut], wv[cut]], axis=1))
        total = term if total is None else total + term
    for load in wq_loads:
        load.start()
    for k in order:
        wo_loads[k].start()
    packed = total.astype(jnp.bfloat16).reshape(own, KB, width)
    local[...] = packed
    pool[pl.ds(0, own)] = packed
    first = own + me * HOT_MOST
    for r in range(HOT_MOST):
        pool[first + r] = local[mine[r]]
    pl.semaphore_wait(barrier, half + n_tp - 1)

    def give(source, device, send):
        rows = pl.ds(own + source * HOT_MOST, HOT_MOST)
        return pltpu.make_async_remote_copy(
            src_ref=pool.at[rows],
            dst_ref=pool.at[rows],
            send_sem=send,
            recv_sem=hot_recv.at[source],
            device_id=(device, t),
            device_id_type=MESH,
        )

    def send_own(j, carry):
        give(me, lax.rem(me + 2 * j, n), hot_send.at[j]).start()
        return carry

    lax.fori_loop(1, half, send_own, 0)
    give(me, partner, hot_send.at[0]).start()

    for i in range(wq.shape[0]):
        wq_loads[i].wait()
        q[:, i * q_chunk : (i + 1) * q_chunk] = dot(x[...], wq[i]).astype(jnp.bfloat16)

    def pass_on(j, carry):
        source = lax.rem(me + n - 2 * j, n)
        copy = give(source, partner, pass_send.at[j])
        copy.wait_recv()
        copy.start()
        return carry

    lax.fori_loop(1, half, pass_on, 0)

    def land(j, carry):
        source = lax.rem(partner + n - 2 * j, n)
        give(source, partner, pass_send.at[0]).wait_recv()
        return carry

    lax.fori_loop(0, half, land, 0)
    for k in range(1, n_tp):
        wo_loads[k].wait()

    low = lax.broadcasted_iota(jnp.int32, (keys, LANES), 1) < HD
    zero = jnp.zeros((keys, LANES), jnp.bfloat16)
    ones = jnp.ones((keys, LANES), jnp.bfloat16)
    ones_low, ones_high = jnp.where(low, ones, zero), jnp.where(low, zero, ones)
    lane = lax.broadcasted_iota(jnp.int32, (1, keys), 1)
    in_block = lax.rem(lane, KB)
    entry_of = lax.div(lane, KB)

    def part_copy(k, b):
        at = (k - 1) * blocks + b
        return pltpu.make_async_remote_copy(
            src_ref=sent.at[k - 1, b],
            dst_ref=got_hbm.at[k - 1, b],
            send_sem=part_send.at[at],
            recv_sem=part_recv.at[at],
            device_id=(me, targets[k]),
            device_id_type=MESH,
        )

    def attend(b, carry):
        key_pos = in_block
        for e in range(nsel):
            code = chosen_ref[b, e]
            listed = jnp.clip(code - own, 0, nhot - 1)
            is_own = code < own
            row = jnp.where(is_own, code, slot_ref[listed])
            block_id = jnp.where(is_own, me * own + code, hot_ref[listed])
            kvg[e * KB : (e + 1) * KB, :] = pool[row]
            key_pos = jnp.where(entry_of == e, block_id * KB + in_block, key_pos)
        query_pos = (me * blocks + b) * QB + lax.broadcasted_iota(jnp.int32, (QB, keys), 0)
        bias = jnp.where(key_pos <= query_pos, 0.0, -jnp.inf).astype(jnp.float32)
        rows = pl.ds(pl.multiple_of(b * QB, QB), QB)

        def spread(u):
            tile = kvg[:, (u // 2) * LANES : (u // 2 + 1) * LANES]
            turned = jnp.concatenate([tile[:, HD:], tile[:, :HD]], axis=1)
            if u % 2 == 1:
                tile, turned = turned, tile
            return jnp.where(low, tile, zero), jnp.where(low, zero, turned)

        for c in range(kv_heads):
            k_low, k_high = spread(c)
            k_both = jnp.concatenate([k_low, k_high], axis=0)
            v_low, v_high = spread(kv_heads + c)
            v_both = jnp.concatenate(
                [
                    jnp.concatenate([v_low, ones_low], axis=1),
                    jnp.concatenate([v_high, ones_high], axis=1),
                ],
                axis=0,
            )
            first_pair = c * pairs
            q_rows = jnp.concatenate(
                [
                    q[rows, (first_pair + p) * LANES : (first_pair + p + 1) * LANES]
                    for p in range(pairs)
                ],
                axis=0,
            )
            scores = lax.dot_general(
                q_rows, k_both, (((1,), (1,)), ((), ())), preferred_element_type=jnp.float32
            )
            lifted = []
            for p in range(pairs):
                both = []
                for s in range(2):
                    factor = scale_ref[(first_pair + p) * 2 + s] * (HD**-0.5 * LOG2E)
                    part = scores[p * QB : (p + 1) * QB, s * keys : (s + 1) * keys]
                    part = part * factor + bias
                    top = jnp.max(part, axis=1, keepdims=True)
                    both.append(jnp.exp2(part - top).astype(jnp.bfloat16))
                lifted.append(jnp.concatenate(both, axis=1))
            summed = dot(jnp.concatenate(lifted, axis=0), v_both)
            held = (summed[:, :LANES] / summed[:, LANES:]).astype(jnp.bfloat16)
            for p in range(pairs):
                heads[rows, (first_pair + p) * LANES : (first_pair + p + 1) * LANES] = held[
                    p * QB : (p + 1) * QB
                ]
        for k in range(1, n_tp):
            sent[k - 1, b] = dot(heads[rows, :], wo[k]).astype(jnp.bfloat16)
            part_copy(k, b).start()
        return carry

    lax.fori_loop(0, blocks, attend, 0)

    wo_loads[0].wait()
    mine_part[...] = dot(heads[...], wo[0]).astype(jnp.bfloat16)
    keep = pltpu.make_async_copy(mine_part, mine_hbm, load_sem.at[0])
    keep.start()
    keep.wait()

    def drain(b, carry):
        for k in range(1, n_tp):
            part_copy(k, b).wait()
        return carry

    lax.fori_loop(0, blocks, drain, 0)

    def drain_hot(j, carry):
        give(me, partner, hot_send.at[j]).wait_send()
        return carry

    lax.fori_loop(0, half, drain_hot, 0)

    def drain_pass(j, carry):
        give(me, partner, pass_send.at[j]).wait_send()
        return carry

    lax.fori_loop(1, half, drain_pass, 0)


def solution(mesh):
    n, n_tp = mesh.shape["kv"], mesh.shape["tp"]

    def local(x, wq, wk, wv, wo, scale, hot, chosen):
        tok, depth = x.shape
        own = tok // KB
        width = wk.shape[1] + wv.shape[1]
        blocks, nsel = chosen.shape
        q_cols = wq.shape[1]
        q_chunk = 256
        part_cols = wo.shape[1] // n_tp
        bf16 = jnp.bfloat16
        dma = pltpu.SemaphoreType.DMA
        any_space = pl.BlockSpec(memory_space=pl.ANY)
        smem = pl.BlockSpec(memory_space=pltpu.SMEM)
        mine, got = pl.pallas_call(
            functools.partial(kernel, n, n_tp),
            out_shape=[
                jax.ShapeDtypeStruct((tok, part_cols), bf16),
                jax.ShapeDtypeStruct((n_tp - 1, blocks, QB, part_cols), bf16),
            ],
            in_specs=[any_space] * 5 + [smem] * 3,
            out_specs=[any_space] * 2,
            scratch_shapes=[
                pltpu.VMEM((tok, depth), bf16),
                pltpu.VMEM((q_cols // q_chunk, depth, q_chunk), bf16),
                pltpu.VMEM(wk.shape, bf16),
                pltpu.VMEM(wv.shape, bf16),
                pltpu.VMEM((n_tp, wo.shape[0], part_cols), bf16),
                pltpu.VMEM((tok, q_cols), bf16),
                pltpu.VMEM((own, KB, width), bf16),
                pltpu.VMEM((own + HOT_MOST * n, KB, width), bf16),
                pltpu.VMEM((nsel * KB, width), bf16),
                pltpu.VMEM((tok, q_cols), bf16),
                pltpu.VMEM((n_tp - 1, blocks, QB, part_cols), bf16),
                pltpu.VMEM((tok, part_cols), bf16),
                pltpu.SMEM(hot.shape, jnp.int32),
                dma((3 * PIECES,)),
                dma((q_cols // q_chunk,)),
                dma((n_tp,)),
                dma((n // 2,)),
                dma((n // 2,)),
                dma((n,)),
                dma(((n_tp - 1) * blocks,)),
                dma(((n_tp - 1) * blocks,)),
            ],
            compiler_params=pltpu.CompilerParams(
                collective_id=0, has_side_effects=True, vmem_limit_bytes=60 * 1024 * 1024
            ),
        )(x, wq, wk, wv, wo, scale, hot, chosen)
        total = mine.astype(jnp.float32)
        for k in range(n_tp - 1):
            total = total + got[k].reshape(tok, part_cols).astype(jnp.float32)
        return total.astype(bf16)

    return jax.shard_map(
        local,
        mesh=mesh,
        in_specs=(
            P("kv", None),
            P(None, "tp"),
            P(None, "tp"),
            P(None, "tp"),
            P("tp", None),
            P("tp"),
            P(),
            P("kv", None),
        ),
        out_specs=P("kv", "tp"),
        check_vma=False,
    )
```

profile of v0, /device:TPU:0, one launch (start us, length us, event | category | flops | bytes accessed | tf_op | source)
XLA Modules:
  0.0 37.3 jit_solution(11232566796900672955)
XLA Ops:
  0.0 34.8 %shard_map.82 = (bf16[384,1024]{1,0:T(8,128)(2,1)}, bf16[1,6,64,1024]{3,2,1,0:T(8,128)(2,1)}) custom-call(bf16[384,2048]{1,0:T(8,128)(2,1)} %x_hbm.1, bf16[2048,1024]{1,0:T(8,128)(2,1)} %wq_hbm.1, bf16[2048,128]{1,0:T(8,128)(2,1)} %wk_hbm.1, bf16[2048,128]{1,0:T(8,128)(2,1)} %wv_hbm.1, bf16[1024,2048]{1,0:T(8,128)(2,1)} %wo_hbm.1, f32[16]{0:T(128)} %scale_ref.1, ...), custom_call_target="tpu_custom_call" | custom-call | tf_op jit(solution)/shard_map/pallas_call | solution.py:312
  34.8 2.6 %fusion = bf16[384,1024]{1,0:T(8,128)(2,1)} fusion(bf16[384,1024]{1,0:T(8,128)(2,1)} %get-tuple-element.7, bf16[1,6,64,1024]{3,2,1,0:T(8,128)(2,1)} %get-tuple-element.8), kind=kLoop, calls=%fused_computation.1 | loop fusion | flops 1572864 | bytes 2359296 | tf_op jit(solution)/shard_map/convert_element_type | solution.py:350
where the time goes:
time: 37.5 us; the launch traced here: 37.3 us
  Pallas kernels  34.8 us (93%)
  other arithmetic  2.56 us (7%)
    pallas_call x1, Pallas kernels, local(): pl.pallas_call(functools.partial(kernel, n, n_tp), out_shape=[jax.ShapeDt...  34.8 us
    convert_element_type x1, other arithmetic, local(): return total.astype(bf16)  2.56 us

commit v1 on v0

--- a/solution.py
+++ b/solution.py
@@ -29,11 +29,10 @@
     wk_hbm,
     wv_hbm,
     wo_hbm,
-    scale_ref,
-    hot_ref,
-    chosen_ref,
-    mine_hbm,
-    got_hbm,
+    scale_hbm,
+    hot_hbm,
+    chosen_hbm,
+    out,
     x,
     wq,
     wk,
@@ -45,8 +44,14 @@
     kvg,
     heads,
     sent,
+    got,
     mine_part,
+    bias,
+    scale_ref,
+    hot_ref,
+    chosen_ref,
     slot_ref,
+    small_sem,
     load_sem,
     wq_sem,
     wo_sem,
@@ -81,7 +86,16 @@
         ]
         for i, cut in enumerate(cuts)
     ]
-    for piece in loads:
+    smalls = [
+        pltpu.make_async_copy(hot_hbm, hot_ref, small_sem.at[0]),
+        pltpu.make_async_copy(chosen_hbm, chosen_ref, small_sem.at[1]),
+        pltpu.make_async_copy(scale_hbm, scale_ref, small_sem.at[2]),
+    ]
+    for load in loads[0]:
+        load.start()
+    for small in smalls:
+        small.start()
+    for piece in loads[1:]:
         for load in piece:
             load.start()
     q_chunk = wq.shape[2]
@@ -113,6 +127,8 @@
     for k in range(1, n_tp):
         pl.semaphore_signal(barrier, inc=1, device_id=(me, targets[k]), device_id_type=MESH)
 
+    for small in smalls:
+        small.wait()
     hots = [hot_ref[h] for h in range(nhot)]
     owners = [lax.div(hot, own) for hot in hots]
     mine = [jnp.int32(0), jnp.int32(0)]
@@ -129,12 +145,13 @@
     for piece, cut in zip(loads, cuts):
         for load in piece:
             load.wait()
+        if total is None:
+            for load in wq_loads:
+                load.start()
+            for k in order:
+                wo_loads[k].start()
         term = dot(x[:, cut], jnp.concatenate([wk[cut], wv[cut]], axis=1))
         total = term if total is None else total + term
-    for load in wq_loads:
-        load.start()
-    for k in order:
-        wo_loads[k].start()
     packed = total.astype(jnp.bfloat16).reshape(own, KB, width)
     local[...] = packed
     pool[pl.ds(0, own)] = packed
@@ -165,6 +182,23 @@
         wq_loads[i].wait()
         q[:, i * q_chunk : (i + 1) * q_chunk] = dot(x[...], wq[i]).astype(jnp.bfloat16)
 
+    lane = lax.broadcasted_iota(jnp.int32, (1, keys), 1)
+    in_block = lax.rem(lane, KB)
+    entry_of = lax.div(lane, KB)
+
+    def mask(b, carry):
+        key_pos = in_block
+        for e in range(nsel):
+            code = chosen_ref[b, e]
+            listed = jnp.clip(code - own, 0, nhot - 1)
+            block_id = jnp.where(code < own, me * own + code, hot_ref[listed])
+            key_pos = jnp.where(entry_of == e, block_id * KB + in_block, key_pos)
+        query_pos = (me * blocks + b) * QB + lax.broadcasted_iota(jnp.int32, (QB, keys), 0)
+        bias[b] = jnp.where(key_pos <= query_pos, 0.0, -jnp.inf).astype(jnp.float32)
+        return carry
+
+    lax.fori_loop(0, blocks, mask, 0)
+
     def pass_on(j, carry):
         source = lax.rem(me + n - 2 * j, n)
         copy = give(source, partner, pass_send.at[j])
@@ -187,15 +221,12 @@
     zero = jnp.zeros((keys, LANES), jnp.bfloat16)
     ones = jnp.ones((keys, LANES), jnp.bfloat16)
     ones_low, ones_high = jnp.where(low, ones, zero), jnp.where(low, zero, ones)
-    lane = lax.broadcasted_iota(jnp.int32, (1, keys), 1)
-    in_block = lax.rem(lane, KB)
-    entry_of = lax.div(lane, KB)
 
     def part_copy(k, b):
         at = (k - 1) * blocks + b
         return pltpu.make_async_remote_copy(
             src_ref=sent.at[k - 1, b],
-            dst_ref=got_hbm.at[k - 1, b],
+            dst_ref=got.at[k - 1, b],
             send_sem=part_send.at[at],
             recv_sem=part_recv.at[at],
             device_id=(me, targets[k]),
@@ -203,17 +234,11 @@
         )
 
     def attend(b, carry):
-        key_pos = in_block
         for e in range(nsel):
             code = chosen_ref[b, e]
             listed = jnp.clip(code - own, 0, nhot - 1)
-            is_own = code < own
-            row = jnp.where(is_own, code, slot_ref[listed])
-            block_id = jnp.where(is_own, me * own + code, hot_ref[listed])
+            row = jnp.where(code < own, code, slot_ref[listed])
             kvg[e * KB : (e + 1) * KB, :] = pool[row]
-            key_pos = jnp.where(entry_of == e, block_id * KB + in_block, key_pos)
-        query_pos = (me * blocks + b) * QB + lax.broadcasted_iota(jnp.int32, (QB, keys), 0)
-        bias = jnp.where(key_pos <= query_pos, 0.0, -jnp.inf).astype(jnp.float32)
         rows = pl.ds(pl.multiple_of(b * QB, QB), QB)
 
         def spread(u):
@@ -251,7 +276,7 @@
                 for s in range(2):
                     factor = scale_ref[(first_pair + p) * 2 + s] * (HD**-0.5 * LOG2E)
                     part = scores[p * QB : (p + 1) * QB, s * keys : (s + 1) * keys]
-                    part = part * factor + bias
+                    part = part * factor + bias[b]
                     top = jnp.max(part, axis=1, keepdims=True)
                     both.append(jnp.exp2(part - top).astype(jnp.bfloat16))
                 lifted.append(jnp.concatenate(both, axis=1))
@@ -270,16 +295,17 @@
 
     wo_loads[0].wait()
     mine_part[...] = dot(heads[...], wo[0]).astype(jnp.bfloat16)
-    keep = pltpu.make_async_copy(mine_part, mine_hbm, load_sem.at[0])
-    keep.start()
-    keep.wait()
-
-    def drain(b, carry):
+
+    def finish(b, carry):
+        rows = pl.ds(pl.multiple_of(b * QB, QB), QB)
+        total = mine_part[rows, :].astype(jnp.float32)
         for k in range(1, n_tp):
             part_copy(k, b).wait()
-        return carry
-
-    lax.fori_loop(0, blocks, drain, 0)
+            total = total + got[k - 1, b].astype(jnp.float32)
+        out[rows, :] = total.astype(jnp.bfloat16)
+        return carry
+
+    lax.fori_loop(0, blocks, finish, 0)
 
     def drain_hot(j, carry):
         give(me, partner, hot_send.at[j]).wait_send()
@@ -308,15 +334,12 @@
         bf16 = jnp.bfloat16
         dma = pltpu.SemaphoreType.DMA
         any_space = pl.BlockSpec(memory_space=pl.ANY)
-        smem = pl.BlockSpec(memory_space=pltpu.SMEM)
-        mine, got = pl.pallas_call(
+        vmem = pl.BlockSpec(memory_space=pltpu.VMEM)
+        return pl.pallas_call(
             functools.partial(kernel, n, n_tp),
-            out_shape=[
-                jax.ShapeDtypeStruct((tok, part_cols), bf16),
-                jax.ShapeDtypeStruct((n_tp - 1, blocks, QB, part_cols), bf16),
-            ],
-            in_specs=[any_space] * 5 + [smem] * 3,
-            out_specs=[any_space] * 2,
+            out_shape=pltpu.VMEM((tok, part_cols), bf16),
+            in_specs=[any_space] * 8,
+            out_specs=vmem,
             scratch_shapes=[
                 pltpu.VMEM((tok, depth), bf16),
                 pltpu.VMEM((q_cols // q_chunk, depth, q_chunk), bf16),
@@ -329,8 +352,14 @@
                 pltpu.VMEM((nsel * KB, width), bf16),
                 pltpu.VMEM((tok, q_cols), bf16),
                 pltpu.VMEM((n_tp - 1, blocks, QB, part_cols), bf16),
+                pltpu.VMEM((n_tp - 1, blocks, QB, part_cols), bf16),
                 pltpu.VMEM((tok, part_cols), bf16),
+                pltpu.VMEM((blocks, QB, nsel * KB), jnp.float32),
+                pltpu.SMEM(scale.shape, jnp.float32),
                 pltpu.SMEM(hot.shape, jnp.int32),
+                pltpu.SMEM(chosen.shape, jnp.int32),
+                pltpu.SMEM(hot.shape, jnp.int32),
+                dma((3,)),
                 dma((3 * PIECES,)),
                 dma((q_cols // q_chunk,)),
                 dma((n_tp,)),
@@ -341,14 +370,9 @@
                 dma(((n_tp - 1) * blocks,)),
             ],
             compiler_params=pltpu.CompilerParams(
-                collective_id=0, has_side_effects=True, vmem_limit_bytes=60 * 1024 * 1024
+                collective_id=0, has_side_effects=True, vmem_limit_bytes=32 * 1024 * 1024
             ),
-        )(x, wq, wk, wv, wo, scale, hot, chosen)
-        total = mine.astype(jnp.float32)
-        for k in range(n_tp - 1):
-            total = total + got[k].reshape(tok, part_cols).astype(jnp.float32)
-        return total.astype(bf16)
-
+        )(*[pltpu.with_memory_space_constraint(a, pltpu.HBM) for a in (x, wq, wk, wv, wo, scale, hot, chosen)])
     return jax.shard_map(
         local,
         mesh=mesh,

time: 37.5 us -> 35 us (0.933)
  other arithmetic: 2.56 us -> 0 us
  local copies, waits for them, and re-layouts: 0 us -> 0.88 us
  Pallas kernels: 34.8 us -> 34 us
    convert_element_type x1 -> x0, other arithmetic: 2.56 us -> none  [local(): return total.astype(bf16)]
    unnamed x0 -> x1, local copies, waits for them, and re-layouts: none -> 0.88 us
    pallas_call x1, Pallas kernels: 34.8 us -> 34 us  [local(): pl.pallas_call(functools.partial(kernel, n, n_tp), out_shape=pltpu.VMEM((...]
where the time goes in v1:
time: 35 us; the launch traced here: 34.9 us
  Pallas kernels  34 us (97%)
  local copies, waits for them, and re-layouts  0.88 us (3%)
    pallas_call x1, Pallas kernels, local(): pl.pallas_call(functools.partial(kernel, n, n_tp), out_shape=pltpu.VMEM((...  34 us
    unnamed x1, local copies, waits for them, and re-layouts  0.88 us

profile of v1, /device:TPU:0, one launch (start us, length us, event | category | flops | bytes accessed | tf_op | source)
XLA Modules:
  0.0 34.9 jit_solution(10369609793923252618)
XLA Ops:
  0.0 34.0 %shard_map.82 = bf16[384,1024]{1,0:T(8,128)(2,1)S(1)} custom-call(bf16[384,2048]{1,0:T(8,128)(2,1)} %x_hbm.1, bf16[2048,1024]{1,0:T(8,128)(2,1)} %wq_hbm.1, bf16[2048,128]{1,0:T(8,128)(2,1)} %wk_hbm.1, bf16[2048,128]{1,0:T(8,128)(2,1)} %wv_hbm.1, bf16[1024,2048]{1,0:T(8,128)(2,1)} %wo_hbm.1, f32[16]{0:T(128)} %scale_hbm.1, s32[16]{0:T(128)} %hot_hbm.1, ...), custom_call_target="tpu_custom_call" | custom-call | tf_op jit(solution)/shard_map/pallas_call | solution.py:338
  34.0 0.9 %copy.10 = bf16[384,1024]{1,0:T(8,128)(2,1)} copy(bf16[384,1024]{1,0:T(8,128)(2,1)S(1)} %shard_map.82) | data formatting | bytes 1572864

commit v2 on v1

--- a/solution.py
+++ b/solution.py
@@ -11,6 +11,7 @@
 KB = 32
 QB = 64
 HOT_MOST = 2
+SEND_LEAD = 2
 LANES = 128
 PIECES = 4
 LOG2E = 1.4426950408889634
@@ -21,9 +22,20 @@
     return jnp.dot(a, b, preferred_element_type=jnp.float32)
 
 
+def row_of_chips(mesh, n):
+    where = [tuple(getattr(d, "coords", ())) for d in mesh.devices.reshape(n, -1)[:, 0]]
+    if len(where[0]) != 3:
+        return 1
+    last = [k for k in range(n) if where[k][2] == where[0][2]]
+    wide = len(last) // 2
+    even = last == list(range(len(last))) and wide > 0 and n % (2 * wide) == 0
+    return wide if even else 1
+
+
 def kernel(
     n,
     n_tp,
+    wide,
     x_hbm,
     wq_hbm,
     wk_hbm,
@@ -60,6 +72,8 @@
     hot_recv,
     part_send,
     part_recv,
+    relay_send,
+    ready,
 ):
     me = lax.axis_index("kv")
     t = lax.axis_index("tp")
@@ -116,30 +130,66 @@
 
     barrier = pltpu.get_barrier_semaphore()
 
+    rank = lax.div(me, 2)
+    core = lax.rem(me, 2)
+    level = lax.div(rank, wide)
+    place = lax.rem(rank, wide)
+    top = half // wide - 1
+    below = jnp.where(level == top, rank, level + place)
+
+    def across(chip):
+        return (2 * chip + 1 - core, t)
+
+    def direct(low, high):
+        high_level = lax.div(high, wide)
+        return (
+            (high_level == top)
+            | (high_level == lax.div(low, wide))
+            | (lax.rem(high, wide) == lax.rem(low, wide))
+        )
+
     def greet(j, carry):
-        pl.semaphore_signal(
-            barrier, inc=1, device_id=(lax.rem(me + 2 * j, n), t), device_id_type=MESH
-        )
-        return carry
-
-    lax.fori_loop(1, half, greet, 0)
+        @pl.when(direct(rank, rank + j))
+        def _():
+            pl.semaphore_signal(
+                barrier, inc=1, device_id=across(rank + j), device_id_type=MESH
+            )
+
+        return carry
+
+    lax.fori_loop(1, half - rank, greet, 0)
     pl.semaphore_signal(barrier, inc=1, device_id=(partner, t), device_id_type=MESH)
     for k in range(1, n_tp):
         pl.semaphore_signal(barrier, inc=1, device_id=(me, targets[k]), device_id_type=MESH)
 
+
+    def tell(j, carry):
+        @pl.when(direct(rank - j, rank))
+        def _():
+            pl.semaphore_signal(
+                ready.at[j], inc=1, device_id=across(rank - j), device_id_type=MESH
+            )
+
+        return carry
+
+    def meet():
+        pl.semaphore_wait(barrier, below + n_tp)
+        lax.fori_loop(1, rank + 1, tell, 0)
+
+    pl.when(level > 0)(meet)
     for small in smalls:
         small.wait()
     hots = [hot_ref[h] for h in range(nhot)]
     owners = [lax.div(hot, own) for hot in hots]
     mine = [jnp.int32(0), jnp.int32(0)]
     for h in range(nhot):
-        rank = jnp.int32(0)
+        turn = jnp.int32(0)
         for g in range(h):
-            rank = rank + (owners[g] == owners[h]).astype(jnp.int32)
-        slot_ref[h] = own + owners[h] * HOT_MOST + rank
+            turn = turn + (owners[g] == owners[h]).astype(jnp.int32)
+        slot_ref[h] = jnp.where(lax.div(owners[h], 2) > rank, 0, own + owners[h] * HOT_MOST + turn)
         offset = hots[h] - owners[h] * own
         for r in range(HOT_MOST):
-            mine[r] = jnp.where((owners[h] == me) & (rank == r), offset, mine[r])
+            mine[r] = jnp.where((owners[h] == me) & (turn == r), offset, mine[r])
 
     total = None
     for piece, cut in zip(loads, cuts):
@@ -158,7 +208,6 @@
     first = own + me * HOT_MOST
     for r in range(HOT_MOST):
         pool[first + r] = local[mine[r]]
-    pl.semaphore_wait(barrier, half + n_tp - 1)
 
     def give(source, device, send):
         rows = pl.ds(own + source * HOT_MOST, HOT_MOST)
@@ -171,16 +220,25 @@
             device_id_type=MESH,
         )
 
+    pl.when(level == 0)(meet)
+    give(me, partner, hot_send.at[0]).start()
+    pieces = wq.shape[0]
+
     def send_own(j, carry):
-        give(me, lax.rem(me + 2 * j, n), hot_send.at[j]).start()
-        return carry
-
-    lax.fori_loop(1, half, send_own, 0)
-    give(me, partner, hot_send.at[0]).start()
-
-    for i in range(wq.shape[0]):
-        wq_loads[i].wait()
-        q[:, i * q_chunk : (i + 1) * q_chunk] = dot(x[...], wq[i]).astype(jnp.bfloat16)
+        @pl.when(direct(rank, rank + j))
+        def _():
+            pl.semaphore_wait(ready.at[j], 1)
+            give(me, across(rank + j)[0], hot_send.at[j]).start()
+
+        return carry
+
+    def send_some(stage, begin):
+        part = (half - 1) * (stage + SEND_LEAD) // (SEND_LEAD + 2)
+        upto = jnp.maximum(jnp.minimum(part, half - 1 - rank) + 1, begin)
+        lax.fori_loop(begin, upto, send_own, 0)
+        return upto
+
+    sent_to = send_some(0, jnp.int32(1))
 
     lane = lax.broadcasted_iota(jnp.int32, (1, keys), 1)
     in_block = lax.rem(lane, KB)
@@ -199,21 +257,45 @@
 
     lax.fori_loop(0, blocks, mask, 0)
 
-    def pass_on(j, carry):
-        source = lax.rem(me + n - 2 * j, n)
-        copy = give(source, partner, pass_send.at[j])
+    def relay(j, m):
+        mate = level * wide + lax.rem(place + m, wide)
+        return give(across(rank - j * wide)[0], 2 * mate + core, relay_send.at[j * wide + m])
+
+    def pass_on(j):
+        copy = give(across(rank - j)[0], partner, pass_send.at[j])
         copy.wait_recv()
         copy.start()
-        return carry
-
-    lax.fori_loop(1, half, pass_on, 0)
+
+    def pass_column(j, carry):
+        pass_on(j * wide)
+        for m in range(1, wide):
+            relay(j, m).start()
+        return carry
+
+    def pass_rest(j, carry):
+        pl.when((level == top) | (lax.rem(j, wide) != 0))(lambda: pass_on(j))
+        return carry
+
+    columns = jnp.where(level == top, 0, level)
+    done = jnp.int32(1)
+    for i in range(pieces):
+        wq_loads[i].wait()
+        q[:, i * q_chunk : (i + 1) * q_chunk] = dot(x[...], wq[i]).astype(jnp.bfloat16)
+        if i < 2:
+            sent_to = send_some(i + 1, sent_to)
+        if i == 1:
+            lax.fori_loop(1, columns + 1, pass_column, 0)
+        if i >= 2:
+            upto = lax.div(rank * (i - 1), pieces - 2) + 1
+            lax.fori_loop(done, upto, pass_rest, 0)
+            done = upto
 
     def land(j, carry):
-        source = lax.rem(partner + n - 2 * j, n)
-        give(source, partner, pass_send.at[0]).wait_recv()
-        return carry
-
-    lax.fori_loop(0, half, land, 0)
+        give(2 * (rank - j) + core, partner, pass_send.at[0]).wait_recv()
+        return carry
+
+    give(partner, partner, pass_send.at[0]).wait_recv()
+    lax.fori_loop(1, rank + 1, land, 0)
     for k in range(1, n_tp):
         wo_loads[k].wait()
 
@@ -307,21 +389,34 @@
 
     lax.fori_loop(0, blocks, finish, 0)
 
+    give(me, partner, hot_send.at[0]).wait_send()
+
     def drain_hot(j, carry):
-        give(me, partner, hot_send.at[j]).wait_send()
-        return carry
-
-    lax.fori_loop(0, half, drain_hot, 0)
+        @pl.when(direct(rank, rank + j))
+        def _():
+            give(me, partner, hot_send.at[j]).wait_send()
+
+        return carry
+
+    lax.fori_loop(1, half - rank, drain_hot, 0)
 
     def drain_pass(j, carry):
         give(me, partner, pass_send.at[j]).wait_send()
         return carry
 
-    lax.fori_loop(1, half, drain_pass, 0)
+    lax.fori_loop(1, rank + 1, drain_pass, 0)
+
+    def drain_relay(j, carry):
+        for m in range(1, wide):
+            relay(j, m).wait_send()
+        return carry
+
+    lax.fori_loop(1, columns + 1, drain_relay, 0)
 
 
 def solution(mesh):
     n, n_tp = mesh.shape["kv"], mesh.shape["tp"]
+    wide = row_of_chips(mesh, n)
 
     def local(x, wq, wk, wv, wo, scale, hot, chosen):
         tok, depth = x.shape
@@ -336,7 +431,7 @@
         any_space = pl.BlockSpec(memory_space=pl.ANY)
         vmem = pl.BlockSpec(memory_space=pltpu.VMEM)
         return pl.pallas_call(
-            functools.partial(kernel, n, n_tp),
+            functools.partial(kernel, n, n_tp, wide),
             out_shape=pltpu.VMEM((tok, part_cols), bf16),
             in_specs=[any_space] * 8,
             out_specs=vmem,
@@ -368,11 +463,19 @@
                 dma((n,)),
                 dma(((n_tp - 1) * blocks,)),
                 dma(((n_tp - 1) * blocks,)),
+                dma((n // 2,)),
+                pltpu.SemaphoreType.REGULAR((n // 2,)),
             ],
             compiler_params=pltpu.CompilerParams(
                 collective_id=0, has_side_effects=True, vmem_limit_bytes=32 * 1024 * 1024
             ),
-        )(*[pltpu.with_memory_space_constraint(a, pltpu.HBM) for a in (x, wq, wk, wv, wo, scale, hot, chosen)])
+        )(
+            *[
+                pltpu.with_memory_space_constraint(a, pltpu.HBM)
+                for a in (x, wq, wk, wv, wo, scale, hot, chosen)
+            ]
+        )
+
     return jax.shard_map(
         local,
         mesh=mesh,

time: 35 us -> 33.5 us (0.957)
  the two profiles are of different devices: /device:TPU:0 before, /device:TPU:17 now
where the time goes in v2:
time: 33.5 us; the launch traced here: 33.3 us
  Pallas kernels  32.4 us (97%)
  local copies, waits for them, and re-layouts  0.88 us (3%)
    pallas_call x1, Pallas kernels, local(): pl.pallas_call(functools.partial(kernel, n, n_tp, wide), out_shape=pltpu....  32.4 us
    unnamed x1, local copies, waits for them, and re-layouts  0.88 us

profile of v2, /device:TPU:17, one launch (start us, length us, event | category | flops | bytes accessed | tf_op | source)
XLA Modules:
  0.0 33.3 jit_solution(10124246922282341086)
XLA Ops:
  0.0 32.4 %shard_map.82 = bf16[384,1024]{1,0:T(8,128)(2,1)S(1)} custom-call(bf16[384,2048]{1,0:T(8,128)(2,1)} %x_hbm.1, bf16[2048,1024]{1,0:T(8,128)(2,1)} %wq_hbm.1, bf16[2048,128]{1,0:T(8,128)(2,1)} %wk_hbm.1, bf16[2048,128]{1,0:T(8,128)(2,1)} %wv_hbm.1, bf16[1024,2048]{1,0:T(8,128)(2,1)} %wo_hbm.1, f32[16]{0:T(128)} %scale_hbm.1, s32[16]{0:T(128)} %hot_hbm.1, ...), custom_call_target="tpu_custom_call" | custom-call | tf_op jit(solution)/shard_map/pallas_call | solution.py:433
  32.4 0.9 %copy.10 = bf16[384,1024]{1,0:T(8,128)(2,1)} copy(bf16[384,1024]{1,0:T(8,128)(2,1)S(1)} %shard_map.82) | data formatting | bytes 1572864

commit v3 on v2

--- a/solution.py
+++ b/solution.py
@@ -10,8 +10,8 @@
 HD = 64
 KB = 32
 QB = 64
+QR = 32
 HOT_MOST = 2
-SEND_LEAD = 2
 LANES = 128
 PIECES = 4
 LOG2E = 1.4426950408889634
@@ -74,6 +74,7 @@
     part_recv,
     relay_send,
     ready,
+    ready_tp,
 ):
     me = lax.axis_index("kv")
     t = lax.axis_index("tp")
@@ -160,7 +161,10 @@
     lax.fori_loop(1, half - rank, greet, 0)
     pl.semaphore_signal(barrier, inc=1, device_id=(partner, t), device_id_type=MESH)
     for k in range(1, n_tp):
-        pl.semaphore_signal(barrier, inc=1, device_id=(me, targets[k]), device_id_type=MESH)
+
+        @pl.when(targets[k] > t)
+        def _(other=targets[k]):
+            pl.semaphore_signal(barrier, inc=1, device_id=(me, other), device_id_type=MESH)
 
 
     def tell(j, carry):
@@ -173,10 +177,18 @@
         return carry
 
     def meet():
-        pl.semaphore_wait(barrier, below + n_tp)
+        pl.semaphore_wait(barrier, below + 1 + t)
         lax.fori_loop(1, rank + 1, tell, 0)
-
-    pl.when(level > 0)(meet)
+        for k in range(1, n_tp):
+
+            @pl.when(targets[k] < t)
+            def _(other=targets[k]):
+                pl.semaphore_signal(
+                    ready_tp.at[t], inc=1, device_id=(me, other), device_id_type=MESH
+                )
+
+
+    pl.when(rank > 0)(meet)
     for small in smalls:
         small.wait()
     hots = [hot_ref[h] for h in range(nhot)]
@@ -220,9 +232,8 @@
             device_id_type=MESH,
         )
 
-    pl.when(level == 0)(meet)
+    pl.when(rank == 0)(meet)
     give(me, partner, hot_send.at[0]).start()
-    pieces = wq.shape[0]
 
     def send_own(j, carry):
         @pl.when(direct(rank, rank + j))
@@ -232,13 +243,8 @@
 
         return carry
 
-    def send_some(stage, begin):
-        part = (half - 1) * (stage + SEND_LEAD) // (SEND_LEAD + 2)
-        upto = jnp.maximum(jnp.minimum(part, half - 1 - rank) + 1, begin)
-        lax.fori_loop(begin, upto, send_own, 0)
-        return upto
-
-    sent_to = send_some(0, jnp.int32(1))
+    first = jnp.where(level == 0, 1, half - rank)
+    lax.fori_loop(1, first, send_own, 0)
 
     lane = lax.broadcasted_iota(jnp.int32, (1, keys), 1)
     in_block = lax.rem(lane, KB)
@@ -277,18 +283,13 @@
         return carry
 
     columns = jnp.where(level == top, 0, level)
-    done = jnp.int32(1)
-    for i in range(pieces):
+    for i in range(wq.shape[0]):
         wq_loads[i].wait()
         q[:, i * q_chunk : (i + 1) * q_chunk] = dot(x[...], wq[i]).astype(jnp.bfloat16)
-        if i < 2:
-            sent_to = send_some(i + 1, sent_to)
-        if i == 1:
+        if i == 0:
+            lax.fori_loop(first, half - rank, send_own, 0)
             lax.fori_loop(1, columns + 1, pass_column, 0)
-        if i >= 2:
-            upto = lax.div(rank * (i - 1), pieces - 2) + 1
-            lax.fori_loop(done, upto, pass_rest, 0)
-            done = upto
+    lax.fori_loop(1, rank + 1, pass_rest, 0)
 
     def land(j, carry):
         give(2 * (rank - j) + core, partner, pass_send.at[0]).wait_recv()
@@ -304,8 +305,16 @@
     ones = jnp.ones((keys, LANES), jnp.bfloat16)
     ones_low, ones_high = jnp.where(low, ones, zero), jnp.where(low, zero, ones)
 
+    steps = sent.shape[1]
+    for k in range(1, n_tp):
+
+        @pl.when(targets[k] > t)
+        def _(other=targets[k]):
+            pl.semaphore_wait(ready_tp.at[other], 1)
+
+
     def part_copy(k, b):
-        at = (k - 1) * blocks + b
+        at = (k - 1) * steps + b
         return pltpu.make_async_remote_copy(
             src_ref=sent.at[k - 1, b],
             dst_ref=got.at[k - 1, b],
@@ -315,13 +324,16 @@
             device_id_type=MESH,
         )
 
-    def attend(b, carry):
+    def attend(step, carry):
+        b = lax.div(step, QB // QR)
+        half_rows = pl.ds(pl.multiple_of(lax.rem(step, QB // QR) * QR, QR), QR)
+        lift = bias[b, half_rows, :]
         for e in range(nsel):
             code = chosen_ref[b, e]
             listed = jnp.clip(code - own, 0, nhot - 1)
             row = jnp.where(code < own, code, slot_ref[listed])
             kvg[e * KB : (e + 1) * KB, :] = pool[row]
-        rows = pl.ds(pl.multiple_of(b * QB, QB), QB)
+        rows = pl.ds(pl.multiple_of(step * QR, QR), QR)
 
         def spread(u):
             tile = kvg[:, (u // 2) * LANES : (u // 2 + 1) * LANES]
@@ -357,8 +369,8 @@
                 both = []
                 for s in range(2):
                     factor = scale_ref[(first_pair + p) * 2 + s] * (HD**-0.5 * LOG2E)
-                    part = scores[p * QB : (p + 1) * QB, s * keys : (s + 1) * keys]
-                    part = part * factor + bias[b]
+                    part = scores[p * QR : (p + 1) * QR, s * keys : (s + 1) * keys]
+                    part = part * factor + lift
                     top = jnp.max(part, axis=1, keepdims=True)
                     both.append(jnp.exp2(part - top).astype(jnp.bfloat16))
                 lifted.append(jnp.concatenate(both, axis=1))
@@ -366,20 +378,20 @@
             held = (summed[:, :LANES] / summed[:, LANES:]).astype(jnp.bfloat16)
             for p in range(pairs):
                 heads[rows, (first_pair + p) * LANES : (first_pair + p + 1) * LANES] = held[
-                    p * QB : (p + 1) * QB
+                    p * QR : (p + 1) * QR
                 ]
         for k in range(1, n_tp):
-            sent[k - 1, b] = dot(heads[rows, :], wo[k]).astype(jnp.bfloat16)
-            part_copy(k, b).start()
-        return carry
-
-    lax.fori_loop(0, blocks, attend, 0)
+            sent[k - 1, step] = dot(heads[rows, :], wo[k]).astype(jnp.bfloat16)
+            part_copy(k, step).start()
+        return carry
+
+    lax.fori_loop(0, steps, attend, 0)
 
     wo_loads[0].wait()
     mine_part[...] = dot(heads[...], wo[0]).astype(jnp.bfloat16)
 
     def finish(b, carry):
-        rows = pl.ds(pl.multiple_of(b * QB, QB), QB)
+        rows = pl.ds(pl.multiple_of(b * QR, QR), QR)
         total = mine_part[rows, :].astype(jnp.float32)
         for k in range(1, n_tp):
             part_copy(k, b).wait()
@@ -387,7 +399,7 @@
         out[rows, :] = total.astype(jnp.bfloat16)
         return carry
 
-    lax.fori_loop(0, blocks, finish, 0)
+    lax.fori_loop(0, steps, finish, 0)
 
     give(me, partner, hot_send.at[0]).wait_send()
 
@@ -424,7 +436,7 @@
         width = wk.shape[1] + wv.shape[1]
         blocks, nsel = chosen.shape
         q_cols = wq.shape[1]
-        q_chunk = 256
+        q_chunk = 512
         part_cols = wo.shape[1] // n_tp
         bf16 = jnp.bfloat16
         dma = pltpu.SemaphoreType.DMA
@@ -446,8 +458,8 @@
                 pltpu.VMEM((own + HOT_MOST * n, KB, width), bf16),
                 pltpu.VMEM((nsel * KB, width), bf16),
                 pltpu.VMEM((tok, q_cols), bf16),
-                pltpu.VMEM((n_tp - 1, blocks, QB, part_cols), bf16),
-                pltpu.VMEM((n_tp - 1, blocks, QB, part_cols), bf16),
+                pltpu.VMEM((n_tp - 1, tok // QR, QR, part_cols), bf16),
+                pltpu.VMEM((n_tp - 1, tok // QR, QR, part_cols), bf16),
                 pltpu.VMEM((tok, part_cols), bf16),
                 pltpu.VMEM((blocks, QB, nsel * KB), jnp.float32),
                 pltpu.SMEM(scale.shape, jnp.float32),
@@ -461,10 +473,11 @@
                 dma((n // 2,)),
                 dma((n // 2,)),
                 dma((n,)),
-                dma(((n_tp - 1) * blocks,)),
-                dma(((n_tp - 1) * blocks,)),
+                dma(((n_tp - 1) * (tok // QR),)),
+                dma(((n_tp - 1) * (tok // QR),)),
                 dma((n // 2,)),
                 pltpu.SemaphoreType.REGULAR((n // 2,)),
+                pltpu.SemaphoreType.REGULAR((n_tp,)),
             ],
             compiler_params=pltpu.CompilerParams(
                 collective_id=0, has_side_effects=True, vmem_limit_bytes=32 * 1024 * 1024

time: 33.5 us -> 32.7 us (0.976)
  Pallas kernels: 32.4 us -> 31.6 us
    pallas_call x1, Pallas kernels: 32.4 us -> 31.6 us  [local(): pl.pallas_call(functools.partial(kernel, n, n_tp, wide), out_shape=pltpu....]
where the time goes in v3:
time: 32.7 us; the launch traced here: 32.5 us
  Pallas kernels  31.6 us (97%)
  local copies, waits for them, and re-layouts  0.88 us (3%)
    pallas_call x1, Pallas kernels, local(): pl.pallas_call(functools.partial(kernel, n, n_tp, wide), out_shape=pltpu....  31.6 us
    unnamed x1, local copies, waits for them, and re-layouts  0.88 us

profile of v3, /device:TPU:17, one launch (start us, length us, event | category | flops | bytes accessed | tf_op | source)
XLA Modules:
  0.0 32.5 jit_solution(18434157689539945941)
XLA Ops:
  0.0 31.6 %shard_map.82 = bf16[384,1024]{1,0:T(8,128)(2,1)S(1)} custom-call(bf16[384,2048]{1,0:T(8,128)(2,1)} %x_hbm.1, bf16[2048,1024]{1,0:T(8,128)(2,1)} %wq_hbm.1, bf16[2048,128]{1,0:T(8,128)(2,1)} %wk_hbm.1, bf16[2048,128]{1,0:T(8,128)(2,1)} %wv_hbm.1, bf16[1024,2048]{1,0:T(8,128)(2,1)} %wo_hbm.1, f32[16]{0:T(128)} %scale_hbm.1, s32[16]{0:T(128)} %hot_hbm.1, ...), custom_call_target="tpu_custom_call" | custom-call | tf_op jit(solution)/shard_map/pallas_call | solution.py:445
  31.6 0.9 %copy.10 = bf16[384,1024]{1,0:T(8,128)(2,1)} copy(bf16[384,1024]{1,0:T(8,128)(2,1)S(1)} %shard_map.82) | data formatting | bytes 1572864

commit v4 on v3

--- a/solution.py
+++ b/solution.py
@@ -204,17 +204,19 @@
             mine[r] = jnp.where((owners[h] == me) & (turn == r), offset, mine[r])
 
     total = None
+    middle = x.shape[0] // 2
     for piece, cut in zip(loads, cuts):
         for load in piece:
             load.wait()
-        if total is None:
+        if piece is loads[0]:
             for load in wq_loads:
                 load.start()
             for k in order:
                 wo_loads[k].start()
-        term = dot(x[:, cut], jnp.concatenate([wk[cut], wv[cut]], axis=1))
-        total = term if total is None else total + term
-    packed = total.astype(jnp.bfloat16).reshape(own, KB, width)
+        both = jnp.concatenate([wk[cut], wv[cut]], axis=1)
+        term = [dot(x[:middle, cut], both), dot(x[middle:, cut], both)]
+        total = term if total is None else [a + b for a, b in zip(total, term)]
+    packed = jnp.concatenate(total, axis=0).astype(jnp.bfloat16).reshape(own, KB, width)
     local[...] = packed
     pool[pl.ds(0, own)] = packed
     first = own + me * HOT_MOST
@@ -243,7 +245,7 @@
 
         return carry
 
-    first = jnp.where(level == 0, 1, half - rank)
+    first = jnp.where(level == 0, jnp.maximum(top * wide - rank, 1), half - rank)
     lax.fori_loop(1, first, send_own, 0)
 
     lane = lax.broadcasted_iota(jnp.int32, (1, keys), 1)
@@ -346,13 +348,10 @@
             k_low, k_high = spread(c)
             k_both = jnp.concatenate([k_low, k_high], axis=0)
             v_low, v_high = spread(kv_heads + c)
-            v_both = jnp.concatenate(
-                [
-                    jnp.concatenate([v_low, ones_low], axis=1),
-                    jnp.concatenate([v_high, ones_high], axis=1),
-                ],
-                axis=0,
-            )
+            v_parts = [
+                jnp.concatenate([v_low, ones_low], axis=1),
+                jnp.concatenate([v_high, ones_high], axis=1),
+            ]
             first_pair = c * pairs
             q_rows = jnp.concatenate(
                 [
@@ -373,8 +372,11 @@
                     part = part * factor + lift
                     top = jnp.max(part, axis=1, keepdims=True)
                     both.append(jnp.exp2(part - top).astype(jnp.bfloat16))
-                lifted.append(jnp.concatenate(both, axis=1))
-            summed = dot(jnp.concatenate(lifted, axis=0), v_both)
+                lifted.append(both)
+            summed = sum(
+                dot(jnp.concatenate([pair[s] for pair in lifted], axis=0), v_parts[s])
+                for s in range(2)
+            )
             held = (summed[:, :LANES] / summed[:, LANES:]).astype(jnp.bfloat16)
             for p in range(pairs):
                 heads[rows, (first_pair + p) * LANES : (first_pair + p + 1) * LANES] = held[

time: 32.7 us -> 31.5 us (0.963)
  Pallas kernels: 31.6 us -> 30.4 us
    pallas_call x1, Pallas kernels: 31.6 us -> 30.4 us  [local(): pl.pallas_call(functools.partial(kernel, n, n_tp, wide), out_shape=pltpu....]
where the time goes in v4:
time: 31.5 us; the launch traced here: 31.3 us
  Pallas kernels  30.4 us (97%)
  local copies, waits for them, and re-layouts  0.88 us (3%)
    pallas_call x1, Pallas kernels, local(): pl.pallas_call(functools.partial(kernel, n, n_tp, wide), out_shape=pltpu....  30.4 us
    unnamed x1, local copies, waits for them, and re-layouts  0.88 us

profile of v4, /device:TPU:17, one launch (start us, length us, event | category | flops | bytes accessed | tf_op | source)
XLA Modules:
  0.0 31.3 jit_solution(15527828825214828379)
XLA Ops:
  0.0 30.4 %shard_map.82 = bf16[384,1024]{1,0:T(8,128)(2,1)S(1)} custom-call(bf16[384,2048]{1,0:T(8,128)(2,1)} %x_hbm.1, bf16[2048,1024]{1,0:T(8,128)(2,1)} %wq_hbm.1, bf16[2048,128]{1,0:T(8,128)(2,1)} %wk_hbm.1, bf16[2048,128]{1,0:T(8,128)(2,1)} %wv_hbm.1, bf16[1024,2048]{1,0:T(8,128)(2,1)} %wo_hbm.1, f32[16]{0:T(128)} %scale_hbm.1, s32[16]{0:T(128)} %hot_hbm.1, ...), custom_call_target="tpu_custom_call" | custom-call | tf_op jit(solution)/shard_map/pallas_call | solution.py:447
  30.4 0.9 %copy.10 = bf16[384,1024]{1,0:T(8,128)(2,1)} copy(bf16[384,1024]{1,0:T(8,128)(2,1)S(1)} %shard_map.82) | data formatting | bytes 1572864

commit v5 on v4

--- a/solution.py
+++ b/solution.py
@@ -65,14 +65,10 @@
     slot_ref,
     small_sem,
     load_sem,
-    wq_sem,
     wo_sem,
-    hot_send,
     pass_send,
     hot_recv,
-    part_send,
     part_recv,
-    relay_send,
     ready,
     ready_tp,
 ):
@@ -115,7 +111,7 @@
             load.start()
     q_chunk = wq.shape[2]
     wq_loads = [
-        pltpu.make_async_copy(wq_hbm.at[:, pl.ds(i * q_chunk, q_chunk)], wq.at[i], wq_sem.at[i])
+        pltpu.make_async_copy(wq_hbm.at[:, pl.ds(i * q_chunk, q_chunk)], wq.at[i], small_sem.at[i])
         for i in range(wq.shape[0])
     ]
     targets = [lax.rem(t + k, n_tp) for k in range(n_tp)]
@@ -159,7 +155,11 @@
         return carry
 
     lax.fori_loop(1, half - rank, greet, 0)
-    pl.semaphore_signal(barrier, inc=1, device_id=(partner, t), device_id_type=MESH)
+
+    @pl.when(core == 1)
+    def _():
+        pl.semaphore_signal(barrier, inc=1, device_id=(partner, t), device_id_type=MESH)
+
     for k in range(1, n_tp):
 
         @pl.when(targets[k] > t)
@@ -177,14 +177,22 @@
         return carry
 
     def meet():
-        pl.semaphore_wait(barrier, below + 1 + t)
+        expected = below + 1 - core + t
+        pl.when(expected > 0)(lambda: pl.semaphore_wait(barrier, expected))
         lax.fori_loop(1, rank + 1, tell, 0)
+
+        @pl.when(core == 0)
+        def _():
+            pl.semaphore_signal(
+                ready.at[0], inc=1, device_id=(partner, t), device_id_type=MESH
+            )
+
         for k in range(1, n_tp):
 
             @pl.when(targets[k] < t)
             def _(other=targets[k]):
                 pl.semaphore_signal(
-                    ready_tp.at[t], inc=1, device_id=(me, other), device_id_type=MESH
+                    ready_tp.at[t - 1], inc=1, device_id=(me, other), device_id_type=MESH
                 )
 
 
@@ -235,13 +243,14 @@
         )
 
     pl.when(rank == 0)(meet)
-    give(me, partner, hot_send.at[0]).start()
+    pl.when(core == 1)(lambda: pl.semaphore_wait(ready.at[0], 1))
+    give(me, partner, load_sem.at[0]).start()
 
     def send_own(j, carry):
         @pl.when(direct(rank, rank + j))
         def _():
             pl.semaphore_wait(ready.at[j], 1)
-            give(me, across(rank + j)[0], hot_send.at[j]).start()
+            give(me, across(rank + j)[0], load_sem.at[j]).start()
 
         return carry
 
@@ -267,10 +276,10 @@
 
     def relay(j, m):
         mate = level * wide + lax.rem(place + m, wide)
-        return give(across(rank - j * wide)[0], 2 * mate + core, relay_send.at[j * wide + m])
+        return give(across(rank - j * wide)[0], 2 * mate + core, load_sem.at[half + (j - 1) * (wide - 1) + m - 1])
 
     def pass_on(j):
-        copy = give(across(rank - j)[0], partner, pass_send.at[j])
+        copy = give(across(rank - j)[0], partner, pass_send.at[j - 1])
         copy.wait_recv()
         copy.start()
 
@@ -285,12 +294,12 @@
         return carry
 
     columns = jnp.where(level == top, 0, level)
+    lax.fori_loop(1, columns + 1, pass_column, 0)
     for i in range(wq.shape[0]):
         wq_loads[i].wait()
         q[:, i * q_chunk : (i + 1) * q_chunk] = dot(x[...], wq[i]).astype(jnp.bfloat16)
         if i == 0:
             lax.fori_loop(first, half - rank, send_own, 0)
-            lax.fori_loop(1, columns + 1, pass_column, 0)
     lax.fori_loop(1, rank + 1, pass_rest, 0)
 
     def land(j, carry):
@@ -307,12 +316,30 @@
     ones = jnp.ones((keys, LANES), jnp.bfloat16)
     ones_low, ones_high = jnp.where(low, ones, zero), jnp.where(low, zero, ones)
 
+    give(me, partner, load_sem.at[0]).wait_send()
+
+    def drain_hot(j, carry):
+        @pl.when(direct(rank, rank + j))
+        def _():
+            give(me, partner, load_sem.at[j]).wait_send()
+
+        return carry
+
+    lax.fori_loop(1, half - rank, drain_hot, 0)
+
+    def drain_relay(j, carry):
+        for m in range(1, wide):
+            relay(j, m).wait_send()
+        return carry
+
+    lax.fori_loop(1, columns + 1, drain_relay, 0)
+
     steps = sent.shape[1]
     for k in range(1, n_tp):
 
         @pl.when(targets[k] > t)
         def _(other=targets[k]):
-            pl.semaphore_wait(ready_tp.at[other], 1)
+            pl.semaphore_wait(ready_tp.at[other - 1], 1)
 
 
     def part_copy(k, b):
@@ -320,7 +347,7 @@
         return pltpu.make_async_remote_copy(
             src_ref=sent.at[k - 1, b],
             dst_ref=got.at[k - 1, b],
-            send_sem=part_send.at[at],
+            send_sem=load_sem.at[at],
             recv_sem=part_recv.at[at],
             device_id=(me, targets[k]),
             device_id_type=MESH,
@@ -392,6 +419,12 @@
     wo_loads[0].wait()
     mine_part[...] = dot(heads[...], wo[0]).astype(jnp.bfloat16)
 
+    def drain_pass(j, carry):
+        give(me, partner, pass_send.at[j - 1]).wait_send()
+        return carry
+
+    lax.fori_loop(1, rank + 1, drain_pass, 0)
+
     def finish(b, carry):
         rows = pl.ds(pl.multiple_of(b * QR, QR), QR)
         total = mine_part[rows, :].astype(jnp.float32)
@@ -402,30 +435,6 @@
         return carry
 
     lax.fori_loop(0, steps, finish, 0)
-
-    give(me, partner, hot_send.at[0]).wait_send()
-
-    def drain_hot(j, carry):
-        @pl.when(direct(rank, rank + j))
-        def _():
-            give(me, partner, hot_send.at[j]).wait_send()
-
-        return carry
-
-    lax.fori_loop(1, half - rank, drain_hot, 0)
-
-    def drain_pass(j, carry):
-        give(me, partner, pass_send.at[j]).wait_send()
-        return carry
-
-    lax.fori_loop(1, rank + 1, drain_pass, 0)
-
-    def drain_relay(j, carry):
-        for m in range(1, wide):
-            relay(j, m).wait_send()
-        return carry
-
-    lax.fori_loop(1, columns + 1, drain_relay, 0)
 
 
 def solution(mesh):
@@ -441,6 +450,8 @@
         q_chunk = 512
         part_cols = wo.shape[1] // n_tp
         bf16 = jnp.bfloat16
+        relays = (n // 2 // wide - 1) * (wide - 1)
+        shared = max(3 * PIECES, n // 2 + relays, (n_tp - 1) * (tok // QR))
         dma = pltpu.SemaphoreType.DMA
         any_space = pl.BlockSpec(memory_space=pl.ANY)
         vmem = pl.BlockSpec(memory_space=pltpu.VMEM)
@@ -468,18 +479,14 @@
                 pltpu.SMEM(hot.shape, jnp.int32),
                 pltpu.SMEM(chosen.shape, jnp.int32),
                 pltpu.SMEM(hot.shape, jnp.int32),
-                dma((3,)),
-                dma((3 * PIECES,)),
-                dma((q_cols // q_chunk,)),
+                dma((max(3, q_cols // q_chunk),)),
+                dma((shared,)),
                 dma((n_tp,)),
-                dma((n // 2,)),
-                dma((n // 2,)),
+                dma((n // 2 - 1,)),
                 dma((n,)),
                 dma(((n_tp - 1) * (tok // QR),)),
-                dma(((n_tp - 1) * (tok // QR),)),
-                dma((n // 2,)),
                 pltpu.SemaphoreType.REGULAR((n // 2,)),
-                pltpu.SemaphoreType.REGULAR((n_tp,)),
+                pltpu.SemaphoreType.REGULAR((max(n_tp - 1, 1),)),
             ],
             compiler_params=pltpu.CompilerParams(
                 collective_id=0, has_side_effects=True, vmem_limit_bytes=32 * 1024 * 1024

time: 31.5 us -> 31.1 us (0.987)
  no operation moved by 1% of the time
where the time goes in v5:
time: 31.1 us; the launch traced here: 31 us
  Pallas kernels  30.1 us (97%)
  local copies, waits for them, and re-layouts  0.88 us (3%)
    pallas_call x1, Pallas kernels, local(): pl.pallas_call(functools.partial(kernel, n, n_tp, wide), out_shape=pltpu....  30.1 us
    unnamed x1, local copies, waits for them, and re-layouts  0.88 us

profile of v5, /device:TPU:17, one launch (start us, length us, event | category | flops | bytes accessed | tf_op | source)
XLA Modules:
  0.0 31.0 jit_solution(13126262913836143701)
XLA Ops:
  0.0 30.1 %shard_map.82 = bf16[384,1024]{1,0:T(8,128)(2,1)S(1)} custom-call(bf16[384,2048]{1,0:T(8,128)(2,1)} %x_hbm.1, bf16[2048,1024]{1,0:T(8,128)(2,1)} %wq_hbm.1, bf16[2048,128]{1,0:T(8,128)(2,1)} %wk_hbm.1, bf16[2048,128]{1,0:T(8,128)(2,1)} %wv_hbm.1, bf16[1024,2048]{1,0:T(8,128)(2,1)} %wo_hbm.1, f32[16]{0:T(128)} %scale_hbm.1, s32[16]{0:T(128)} %hot_hbm.1, ...), custom_call_target="tpu_custom_call" | custom-call | tf_op jit(solution)/shard_map/pallas_call | solution.py:458
  30.1 0.9 %copy.10 = bf16[384,1024]{1,0:T(8,128)(2,1)} copy(bf16[384,1024]{1,0:T(8,128)(2,1)S(1)} %shard_map.82) | data formatting | bytes 1572864

commit v6 on v5

--- a/solution.py
+++ b/solution.py
@@ -11,6 +11,7 @@
 KB = 32
 QB = 64
 QR = 32
+SPAN = 4
 HOT_MOST = 2
 LANES = 128
 PIECES = 4
@@ -342,13 +343,18 @@
             pl.semaphore_wait(ready_tp.at[other - 1], 1)
 
 
-    def part_copy(k, b):
+    bundles = (steps - 1) // SPAN
+    bundled = bundles * SPAN
+    marks = bundles + steps - bundled
+
+    def part_copy(k, b, count=1):
         at = (k - 1) * steps + b
+        mark = jnp.where(b < bundled, lax.div(b, SPAN), b - bundled + bundles)
         return pltpu.make_async_remote_copy(
-            src_ref=sent.at[k - 1, b],
-            dst_ref=got.at[k - 1, b],
+            src_ref=sent.at[k - 1, pl.ds(b, count)],
+            dst_ref=got.at[k - 1, pl.ds(b, count)],
             send_sem=load_sem.at[at],
-            recv_sem=part_recv.at[at],
+            recv_sem=part_recv.at[(k - 1) * marks + mark],
             device_id=(me, targets[k]),
             device_id_type=MESH,
         )
@@ -425,16 +431,34 @@
 
     lax.fori_loop(1, rank + 1, drain_pass, 0)
 
-    def finish(b, carry):
+    def drain_part(b, carry):
+        for k in range(1, n_tp):
+            part_copy(k, b).wait_send()
+        return carry
+
+    def finish(b):
         rows = pl.ds(pl.multiple_of(b * QR, QR), QR)
         total = mine_part[rows, :].astype(jnp.float32)
         for k in range(1, n_tp):
-            part_copy(k, b).wait()
             total = total + got[k - 1, b].astype(jnp.float32)
         out[rows, :] = total.astype(jnp.bfloat16)
-        return carry
-
-    lax.fori_loop(0, steps, finish, 0)
+
+    def finish_bundle(g, carry):
+        for k in range(1, n_tp):
+            part_copy(k, g * SPAN, SPAN).wait_recv()
+        for r in range(SPAN):
+            finish(g * SPAN + r)
+        return carry
+
+    def finish_one(b, carry):
+        for k in range(1, n_tp):
+            part_copy(k, b).wait_recv()
+        finish(b)
+        return carry
+
+    lax.fori_loop(0, bundles, finish_bundle, 0)
+    lax.fori_loop(bundled, steps, finish_one, 0)
+    lax.fori_loop(0, steps, drain_part, 0)
 
 
 def solution(mesh):
@@ -450,6 +474,8 @@
         q_chunk = 512
         part_cols = wo.shape[1] // n_tp
         bf16 = jnp.bfloat16
+        steps = tok // QR
+        marks = (steps - 1) // SPAN + steps - (steps - 1) // SPAN * SPAN
         relays = (n // 2 // wide - 1) * (wide - 1)
         shared = max(3 * PIECES, n // 2 + relays, (n_tp - 1) * (tok // QR))
         dma = pltpu.SemaphoreType.DMA
@@ -484,7 +510,7 @@
                 dma((n_tp,)),
                 dma((n // 2 - 1,)),
                 dma((n,)),
-                dma(((n_tp - 1) * (tok // QR),)),
+                dma(((n_tp - 1) * marks,)),
                 pltpu.SemaphoreType.REGULAR((n // 2,)),
                 pltpu.SemaphoreType.REGULAR((max(n_tp - 1, 1),)),
             ],

time: 31.1 us -> 31.2 us (level)
  no operation moved by 1% of the time
where the time goes in v6:
time: 31.2 us; the launch traced here: 31 us
  Pallas kernels  30.1 us (96%)
  local copies, waits for them, and re-layouts  0.88 us (3%)
    pallas_call x1, Pallas kernels, local(): pl.pallas_call(functools.partial(kernel, n, n_tp, wide), out_shape=pltpu....  30.1 us
    unnamed x1, local copies, waits for them, and re-layouts  0.88 us

profile of v6, /device:TPU:17, one launch (start us, length us, event | category | flops | bytes accessed | tf_op | source)
XLA Modules:
  0.0 31.0 jit_solution(13900684240603418983)
XLA Ops:
  0.0 30.1 %shard_map.82 = bf16[384,1024]{1,0:T(8,128)(2,1)S(1)} custom-call(bf16[384,2048]{1,0:T(8,128)(2,1)} %x_hbm.1, bf16[2048,1024]{1,0:T(8,128)(2,1)} %wq_hbm.1, bf16[2048,128]{1,0:T(8,128)(2,1)} %wk_hbm.1, bf16[2048,128]{1,0:T(8,128)(2,1)} %wv_hbm.1, bf16[1024,2048]{1,0:T(8,128)(2,1)} %wo_hbm.1, f32[16]{0:T(128)} %scale_hbm.1, s32[16]{0:T(128)} %hot_hbm.1, ...), custom_call_target="tpu_custom_call" | custom-call | tf_op jit(solution)/shard_map/pallas_call | solution.py:484
  30.1 0.9 %copy.10 = bf16[384,1024]{1,0:T(8,128)(2,1)} copy(bf16[384,1024]{1,0:T(8,128)(2,1)S(1)} %shard_map.82) | data formatting | bytes 1572864
